TPU v7x, 32 devices: a whole 2x2x4 slice. The times are simulated.
32 devices in a mesh: dp: 4 (over y, x), kv: 4 (over z), tp: 2 (over core).
Axes of the slice: x: 2, y: 2, z: 4, core: 2. Of those that a mesh axis runs over, the one named last changes fastest.
Arguments:
- tokens: bfloat16 [4, 2048, 2048], P('dp', 'kv'), may hold values from -6 to 6
- w_query: bfloat16 [2048, 1024], P(None, 'tp'), as said below
- w_key: bfloat16 [2048, 1024], P(None, 'tp'), as said below
- w_value: bfloat16 [2048, 1024], P(None, 'tp'), may hold values from -0.125 to 0.125
- w_out: bfloat16 [1024, 2048], P('tp'), may hold values from -0.1875 to 0.1875
- chosen: int32 [4, 32, 16], P('dp', 'kv'), may hold values from -1 to 31, as said below
Outputs:
- mixed: bfloat16 [4, 2048, 2048], P('dp', ('kv', 'tp'))
- log_sums: float32 [4, 16, 2048], P('dp', 'tp', 'kv')
Inputs may be any that keep to these rules, and one draw needn't show every extreme that they name: `chosen`: write d = b // 8 and j = b % 8 for query block b. Row b lists b first, then min(15, j + 2 * d) distinct earlier blocks, then -1. Of the blocks that the query blocks of one index d of kv list, at most 2 lie in the positions of any one other index; the first query block of every index d >= 1 lists 2 blocks of index d - 1, and, where it exists, 2 blocks of the index half the sequence earlier. `w_query`: A weight matrix with entries up to about 4. `w_key`: A weight matrix of entries of order 2048 to the power -1/2.
All inputs are finite; a program needn't handle non-finite values.
Results may differ from a plain program's by a relative error of at most 0.0093.
Values may be sent and summed in bfloat16 or wider, within the bound.
A program may use at most 192 MiB of HBM per device.

v0:
```python
import functools

import jax
import jax.numpy as jnp
from jax import lax
from jax.experimental import pallas as pl
from jax.experimental.pallas import tpu as pltpu
from jax.sharding import PartitionSpec as P

HEAD_DIM = 64
BLOCK = 64


def on_device_general(tokens, w_query, w_key, w_value, w_out, chosen):
    inputs = tokens[0]
    listed = chosen[0]
    tok_rows = inputs.shape[0]
    queries = jnp.dot(inputs, w_query, preferred_element_type=jnp.float32).astype(jnp.bfloat16)
    keys_local = jnp.dot(inputs, w_key, preferred_element_type=jnp.float32).astype(jnp.bfloat16)
    values_local = jnp.dot(inputs, w_value, preferred_element_type=jnp.float32).astype(jnp.bfloat16)
    width = queries.shape[1]
    head_count = width // HEAD_DIM
    span_blocks = tok_rows // BLOCK
    query_count, picks = listed.shape
    myself = lax.axis_index("kv")
    valid = listed >= 0
    key_blocks = keys_local.reshape(span_blocks, BLOCK, width)
    value_blocks = values_local.reshape(span_blocks, BLOCK, width)
    kv_count = lax.axis_size("kv")
    capacity = max(1, min(2, span_blocks // 3))
    owners = jnp.where(valid, listed // span_blocks, myself)
    within = jnp.where(valid, listed % span_blocks, 0)
    foreign = valid & (owners != myself)
    owner_iota = jnp.arange(kv_count, dtype=jnp.int32)
    within_iota = jnp.arange(span_blocks, dtype=jnp.int32)
    hits = (
        (owners[:, :, None, None] == owner_iota[:, None])
        & (within[:, :, None, None] == within_iota[None, :])
        & foreign[:, :, None, None]
    )
    needed = jnp.any(hits, axis=(0, 1))
    order_rank = jnp.cumsum(needed.astype(jnp.int32), axis=1) - 1
    matches = needed[:, None, :] & (
        order_rank[:, None, :] == jnp.arange(capacity, dtype=jnp.int32)[None, :, None]
    )
    wanted = jnp.where(
        jnp.any(matches, axis=2), jnp.sum(matches.astype(jnp.int32) * within_iota, axis=2), -1
    )
    asked = lax.all_to_all(wanted, "kv", split_axis=0, concat_axis=0, tiled=True)
    present = (asked >= 0)[:, :, None, None]
    picked = jnp.clip(asked, 0, span_blocks - 1)
    zero_block = jnp.zeros((), jnp.bfloat16)
    send_keys = jnp.where(present, key_blocks[picked], zero_block)
    send_values = jnp.where(present, value_blocks[picked], zero_block)
    got_keys, got_values = (
        lax.all_to_all(send_keys, "kv", split_axis=0, concat_axis=0, tiled=True),
        lax.all_to_all(send_values, "kv", split_axis=0, concat_axis=0, tiled=True),
    )
    pool_keys = jnp.concatenate([key_blocks, got_keys.reshape(-1, BLOCK, width)], axis=0)
    pool_values = jnp.concatenate([value_blocks, got_values.reshape(-1, BLOCK, width)], axis=0)
    slot_rank = jnp.sum(hits.astype(jnp.int32) * order_rank[None, None], axis=(2, 3))
    slots = jnp.where(foreign, span_blocks + owners * capacity + slot_rank, within)
    keys_sel = pool_keys[slots].reshape(query_count, picks, BLOCK, head_count, HEAD_DIM)
    values_sel = pool_values[slots].reshape(query_count, picks, BLOCK, head_count, HEAD_DIM)
    query_blocks = queries.reshape(query_count, BLOCK, head_count, HEAD_DIM)
    scores = jnp.einsum(
        "nqhd,nskhd->nhqsk", query_blocks, keys_sel, preferred_element_type=jnp.float32
    ) * HEAD_DIM ** (-0.5)
    offsets = jnp.arange(BLOCK, dtype=jnp.int32)
    key_pos = listed[:, :, None] * BLOCK + offsets[None, None, :]
    query_pos = (myself * span_blocks + jnp.arange(query_count, dtype=jnp.int32))[
        :, None
    ] * BLOCK + offsets[None, :]
    allowed = valid[:, None, :, None] & (key_pos[:, None, :, :] <= query_pos[:, :, None, None])
    scores = jnp.where(allowed[:, None], scores, -jnp.inf)
    row_max = jnp.max(scores, axis=(3, 4), keepdims=True)
    exp_terms = jnp.exp(scores - row_max)
    row_sum = jnp.sum(exp_terms, axis=(3, 4), keepdims=True)
    weights = (exp_terms / row_sum).astype(jnp.bfloat16)
    attended = jnp.einsum(
        "nhqsk,nskhd->nqhd", weights, values_sel, preferred_element_type=jnp.float32
    )
    attended = attended.astype(jnp.bfloat16).reshape(tok_rows, width)
    log_sums = (row_max + jnp.log(row_sum))[:, :, :, 0, 0]
    log_sums = jnp.transpose(log_sums, (1, 0, 2)).reshape(head_count, tok_rows)
    mixed = lax.psum_scatter(
        jnp.dot(attended, w_out, preferred_element_type=jnp.float32).astype(jnp.bfloat16),
        "tp",
        scatter_dimension=0,
        tiled=True,
    )
    return (mixed[None], log_sums[None])


CAPACITY = 2
LANES = 128
QTILE = 256


def fused_kernel(
    n, tokens_hbm, wq_hbm, wk_hbm, wv_hbm, wo_hbm, chosen_ref, mixed_ref, lse_ref,
    x, wq, wk, wv, wo, q_s, k_s, vt_s, send_k, send_v, got_k, got_v, asked,
    acc, mx, sm, top, inv, far_s, far_e, att, att_far, wo_far, part,
    load_sem, ask_send, ask_recv, kv_send, kv_recv, part_send, part_recv,
):
    me = lax.axis_index("kv")
    core = lax.axis_index("tp")
    rows, width = q_s.shape
    depth = wo.shape[1]
    half = rows // 2
    blocks = rows // BLOCK
    pairs = width // LANES
    foreign_rows = CAPACITY * BLOCK

    loads = []
    for index, (src, dst) in enumerate(
        ((tokens_hbm.at[0], x), (wk_hbm, wk), (wv_hbm, wv), (wq_hbm, wq), (wo_hbm, wo))
    ):
        loads.append(pltpu.make_async_copy(src, dst, load_sem.at[index]))
    loads[0].start()
    loads[1].start()

    barrier = pltpu.get_barrier_semaphore()
    for offset in range(1, n):
        pl.semaphore_signal(
            barrier, inc=1, device_id={"kv": lax.rem(me + offset, n)},
            device_id_type=pl.DeviceIdType.MESH,
        )
    pl.semaphore_signal(
        barrier, inc=1, device_id={"tp": 1 - core}, device_id_type=pl.DeviceIdType.MESH
    )
    pl.semaphore_wait(barrier, n)

    def ask_copy(offset):
        return pltpu.make_async_remote_copy(
            src_ref=chosen_ref, dst_ref=asked.at[offset - 1],
            send_sem=ask_send.at[offset - 1], recv_sem=ask_recv.at[offset - 1],
            device_id={"kv": lax.rem(me + n - offset, n)}, device_id_type=pl.DeviceIdType.MESH,
        )

    def kv_copy(offset, which):
        return pltpu.make_async_remote_copy(
            src_ref=(send_k, send_v)[which].at[offset - 1],
            dst_ref=(got_k, got_v)[which].at[offset - 1],
            send_sem=kv_send.at[which, offset - 1], recv_sem=kv_recv.at[which, offset - 1],
            device_id={"kv": lax.rem(me + offset, n)}, device_id_type=pl.DeviceIdType.MESH,
        )

    for offset in range(1, n):
        @pl.when(me >= offset)
        def _():
            ask_copy(offset).start()

    def project(w, out, scale, turn=False):
        step = 256

        @pl.loop(0, width // step)
        def _(j):
            cols = pl.ds(pl.multiple_of(j * step, step), step)
            y = jnp.dot(x[...], w[:, cols], preferred_element_type=jnp.float32)
            y = y.astype(jnp.bfloat16)
            if turn:
                out[cols, :] = y.T
            else:
                out[:, cols] = y * jnp.asarray(scale, jnp.bfloat16) if scale != 1.0 else y

    def pick(offset):
        row = asked[offset - 1, 0, 0:1, :]
        inside = (row >= me * blocks) & (row < (me + 1) * blocks)
        low = jnp.min(jnp.where(inside, row, (me + 1) * blocks - 1), axis=1, keepdims=True)
        high = jnp.max(jnp.where(inside, row, me * blocks), axis=1, keepdims=True)
        low, high = low - me * blocks, high - me * blocks
        place = lax.broadcasted_iota(jnp.int32, (foreign_rows, rows), 0)
        column = lax.broadcasted_iota(jnp.int32, (foreign_rows, rows), 1)
        want = jnp.where(place < BLOCK, low * BLOCK + place, high * BLOCK + place - BLOCK)
        return (column == want).astype(jnp.float32).astype(jnp.bfloat16)

    def select_and_send(which):
        for offset in range(n - 1, 0, -1):
            @pl.when(me + offset < n)
            def _():
                if which == 0:
                    ask_copy(offset).wait_recv()
                one_hot = pick(offset)
                if which == 0:
                    got = jnp.dot(one_hot, k_s[...], preferred_element_type=jnp.float32)
                else:
                    got = lax.dot_general(
                        vt_s[...], one_hot, (((1,), (1,)), ((), ())), preferred_element_type=jnp.float32
                    )
                (send_k, send_v)[which][offset - 1] = got.astype(jnp.bfloat16)
                kv_copy(offset, which).start()

    loads[0].wait()
    loads[1].wait()
    for load in loads[2:]:
        load.start()
    project(wk, k_s, 1.0)
    select_and_send(0)
    loads[2].wait()
    project(wv, vt_s, 1.0, turn=True)
    select_and_send(1)
    wo_copy = pltpu.make_async_remote_copy(
        src_ref=wo_hbm, dst_ref=wo_far,
        send_sem=part_send.at[1], recv_sem=part_recv.at[1],
        device_id={"tp": 1 - core}, device_id_type=pl.DeviceIdType.MESH,
    )
    wo_copy.start()
    loads[3].wait()
    project(wq, q_s, HEAD_DIM ** (-0.5))

    first = lax.broadcasted_iota(jnp.int32, (rows, LANES), 1) < HEAD_DIM
    zero = jnp.zeros((), jnp.bfloat16)

    def one_head(q, half_of_pair):
        mine = first[: q.shape[0]]
        return jnp.where(mine, q, zero) if half_of_pair == 0 else jnp.where(mine, zero, q)

    def attend(q, k, vt, mask):
        s = lax.dot_general(k, q, (((1,), (1,)), ((), ())), preferred_element_type=jnp.float32)
        if mask is not None:
            last = jnp.where(mask, s[-QTILE:], -jnp.inf)
            s = last if s.shape[0] == QTILE else jnp.concatenate([s[:-QTILE], last], axis=0)
        m = jnp.max(s, axis=0, keepdims=True)
        e = jnp.exp(s - m)
        l = jnp.sum(e, axis=0, keepdims=True)
        o = jnp.dot(vt, e.astype(jnp.bfloat16), preferred_element_type=jnp.float32)
        return m, l, o

    tri = lax.broadcasted_iota(jnp.int32, (QTILE, QTILE), 0) <= lax.broadcasted_iota(
        jnp.int32, (QTILE, QTILE), 1
    )

    @pl.loop(0, pairs)
    def _(p):
        cols = pl.ds(pl.multiple_of(p * LANES, LANES), LANES)
        for i in range(rows // QTILE):
            here = slice(i * QTILE, (i + 1) * QTILE)
            keys = slice(0, (i + 1) * QTILE)
            q, k = q_s[here, cols], k_s[keys, cols]
            for side in range(2):
                head = 2 * p + side
                wide = pl.ds(pl.multiple_of(head * HEAD_DIM, HEAD_DIM), HEAD_DIM)
                m, l, o = attend(one_head(q, side), k, vt_s[wide, keys], tri)
                mx[pl.ds(head, 1), here] = m
                sm[pl.ds(head, 1), here] = l
                acc[wide, here] = o

    def of_head(p, side):
        head = 2 * p + side
        wide = pl.ds(pl.multiple_of(head * HEAD_DIM, HEAD_DIM), HEAD_DIM)
        far = pl.ds(pl.multiple_of(head * foreign_rows, foreign_rows), foreign_rows)
        return pl.ds(head, 1), wide, far

    top[...] = mx[...]
    for offset in range(1, n):
        @pl.when(me >= offset)
        def _():
            kv_copy(offset, 0).wait_recv()

            @pl.loop(0, pairs)
            def _(p):
                cols = pl.ds(pl.multiple_of(p * LANES, LANES), LANES)
                q, k = q_s[:, cols], got_k[offset - 1, :, cols]
                for side in range(2):
                    line, _, far = of_head(p, side)
                    s = lax.dot_general(
                        k, one_head(q, side), (((1,), (1,)), ((), ())),
                        preferred_element_type=jnp.float32,
                    )
                    far_s[offset - 1, far, :] = s
                    top[line, :] = jnp.maximum(top[line, :], jnp.max(s, axis=0, keepdims=True))

    keep = jnp.exp(mx[...] - top[...])
    sm[...] = sm[...] * keep
    for offset in range(1, n):
        @pl.when(me >= offset)
        def _():
            @pl.loop(0, pairs)
            def _(p):
                for side in range(2):
                    line, _, far = of_head(p, side)
                    e = jnp.exp(far_s[offset - 1, far, :] - top[line, :])
                    sm[line, :] = sm[line, :] + jnp.sum(e, axis=0, keepdims=True)
                    far_e[offset - 1, far, :] = e.astype(jnp.bfloat16)

    inv[...] = 1.0 / sm[...]
    lse_ref[0] = top[...] + jnp.log(sm[...])
    mx[...] = keep * inv[...]

    @pl.loop(0, pairs)
    def _(p):
        for side in range(2):
            line, wide, _ = of_head(p, side)
            acc[wide, :] = acc[wide, :] * mx[line, :]

    def finish(cols, first_half):
        for offset in range(1, n):
            @pl.when(me >= offset)
            def _():
                if first_half:
                    kv_copy(offset, 1).wait_recv()

                @pl.loop(0, pairs)
                def _(p):
                    for side in range(2):
                        line, wide, far = of_head(p, side)
                        o = jnp.dot(
                            got_v[offset - 1, wide, :], far_e[offset - 1, far, cols],
                            preferred_element_type=jnp.float32,
                        )
                        acc[wide, cols] = acc[wide, cols] + o * inv[line, cols]

        att[cols, :] = acc[:, cols].astype(jnp.bfloat16).T

    loads[4].wait()
    chunks = 4
    step = depth // chunks
    theirs = pl.ds(pl.multiple_of((1 - core) * half, half), half)
    mine = pl.ds(pl.multiple_of(core * half, half), half)

    att_copy = pltpu.make_async_remote_copy(
        src_ref=att.at[theirs], dst_ref=att_far,
        send_sem=part_send.at[0], recv_sem=part_recv.at[0],
        device_id={"tp": 1 - core}, device_id_type=pl.DeviceIdType.MESH,
    )
    finish(theirs, True)
    att_copy.start()
    finish(mine, False)
    for c in range(chunks):
        cols = slice(c * step, (c + 1) * step)
        part[:, cols] = jnp.dot(
            att[mine, :], wo[:, cols], preferred_element_type=jnp.float32
        ).astype(jnp.bfloat16)
    wo_copy.wait_recv()
    att_copy.wait_recv()
    for c in range(chunks):
        cols = slice(c * step, (c + 1) * step)
        other = jnp.dot(
            att_far[...], wo_far[:, cols], preferred_element_type=jnp.float32
        ).astype(jnp.bfloat16)
        mixed_ref[0, :, cols] = (
            part[:, cols].astype(jnp.float32) + other.astype(jnp.float32)
        ).astype(jnp.bfloat16)

    att_copy.wait_send()
    wo_copy.wait_send()
    for offset in range(1, n):
        @pl.when(me >= offset)
        def _():
            ask_copy(offset).wait_send()

        @pl.when(me + offset < n)
        def _():
            kv_copy(offset, 0).wait_send()
            kv_copy(offset, 1).wait_send()


def on_device_fused(n, tokens, w_query, w_key, w_value, w_out, chosen):
    _, rows, model = tokens.shape
    width = w_query.shape[1]
    depth = w_out.shape[1]
    blocks, picks = chosen.shape[1:]
    foreign_rows = CAPACITY * BLOCK
    heads = width // HEAD_DIM
    bf16, f32 = jnp.bfloat16, jnp.float32
    in_hbm = pl.BlockSpec(memory_space=pltpu.HBM)
    in_vmem = pl.BlockSpec(memory_space=pltpu.VMEM)
    dma = pltpu.SemaphoreType.DMA
    return pl.pallas_call(
        functools.partial(fused_kernel, n),
        out_shape=(
            jax.ShapeDtypeStruct((1, rows // 2, depth), bf16),
            jax.ShapeDtypeStruct((1, width // HEAD_DIM, rows), f32),
        ),
        in_specs=[in_hbm] * 5 + [in_vmem],
        out_specs=(in_vmem, in_vmem),
        scratch_shapes=[
            pltpu.VMEM((rows, model), bf16),
            pltpu.VMEM((model, width), bf16),
            pltpu.VMEM((model, width), bf16),
            pltpu.VMEM((model, width), bf16),
            pltpu.VMEM((width, depth), bf16),
            pltpu.VMEM((rows, width), bf16),
            pltpu.VMEM((rows, width), bf16),
            pltpu.VMEM((width, rows), bf16),
            pltpu.VMEM((n - 1, foreign_rows, width), bf16),
            pltpu.VMEM((n - 1, width, foreign_rows), bf16),
            pltpu.VMEM((n - 1, foreign_rows, width), bf16),
            pltpu.VMEM((n - 1, width, foreign_rows), bf16),
            pltpu.VMEM((n - 1, 1, blocks, picks), jnp.int32),
            pltpu.VMEM((width, rows), f32),
            pltpu.VMEM((heads, rows), f32),
            pltpu.VMEM((heads, rows), f32),
            pltpu.VMEM((heads, rows), f32),
            pltpu.VMEM((heads, rows), f32),
            pltpu.VMEM((n - 1, heads * foreign_rows, rows), f32),
            pltpu.VMEM((n - 1, heads * foreign_rows, rows), bf16),
            pltpu.VMEM((rows, width), bf16),
            pltpu.VMEM((rows // 2, width), bf16),
            pltpu.VMEM((width, depth), bf16),
            pltpu.VMEM((rows // 2, depth), bf16),
            dma((5,)),
            dma((n - 1,)),
            dma((n - 1,)),
            dma((2, n - 1)),
            dma((2, n - 1)),
            dma((2,)),
            dma((2,)),
        ],
        compiler_params=pltpu.CompilerParams(
            collective_id=0, has_side_effects=True, vmem_limit_bytes=53500 * 1024
        ),
    )(tokens, w_query, w_key, w_value, w_out, chosen)


def on_device(tokens, w_query, w_key, w_value, w_out, chosen):
    n, cores = lax.axis_size("kv"), lax.axis_size("tp")
    rows = tokens.shape[1]
    blocks, picks = chosen.shape[1:]
    full_rows = blocks - 1 + CAPACITY * (n - 1) <= picks - 1
    fits = rows % (2 * QTILE) == 0 and w_query.shape[1] % 256 == 0 and blocks >= 3 * CAPACITY
    if full_rows and fits and cores == 2 and n > 1:
        return on_device_fused(n, tokens, w_query, w_key, w_value, w_out, chosen)
    return on_device_general(tokens, w_query, w_key, w_value, w_out, chosen)


def solution(mesh):
    return jax.shard_map(
        on_device,
        mesh=mesh,
        in_specs=(
            P("dp", "kv", None),
            P(None, "tp"),
            P(None, "tp"),
            P(None, "tp"),
            P("tp", None),
            P("dp", "kv", None),
        ),
        out_specs=(P("dp", ("kv", "tp"), None), P("dp", "tp", "kv")),
        check_vma=False,
    )
```

profile of v0, /device:TPU:17, one launch (start us, length us, event | category | flops | bytes accessed | tf_op | source)
XLA Modules:
  0.0 35.1 jit_solution(10101349372584781522)
XLA Ops:
  0.6 0.0 copy-start
  0.6 0.7 %copy-done = s32[1,8,16]{2,1,0:T(8,128)S(1)} copy-done((s32[1,8,16]{2,1,0:T(8,128)S(1)}, s32[1,8,16]{2,1,0:T(8,128)}, u32[]{:S(2)}) %copy-start) | copy-done | bytes 536
  1.3 32.2 %shard_map.77 = (bf16[1,256,2048]{2,1,0:T(8,128)(2,1)S(1)}, f32[1,8,512]{2,1,0:T(8,128)S(1)}) custom-call(bf16[1,512,2048]{2,1,0:T(8,128)(2,1)} %tokens_hbm.1, bf16[2048,512]{1,0:T(8,128)(2,1)} %wq_hbm.1, bf16[2048,512]{1,0:T(8,128)(2,1)} %wk_hbm.1, bf16[2048,512]{1,0:T(8,128)(2,1)} %wv_hbm.1, bf16[512,2048]{1,0:T(8,128)(2,1)} %wo_hbm.1, s32[1,8,16]{2,1,0:T(8,128)S(1)} %copy-done), custom_call_target="tpu_custom_call" | custom-call | tf_op jit(solution)/shard_map/pallas_call | solution.py:370
  33.5 1.0 %copy.10 = bf16[1,256,2048]{2,1,0:T(8,128)(2,1)} copy(bf16[1,256,2048]{2,1,0:T(8,128)(2,1)S(1)} %get-tuple-element.4) | data formatting | bytes 2097152
  34.5 0.6 %copy.11 = f32[1,8,512]{2,1,0:T(8,128)} copy(f32[1,8,512]{2,1,0:T(8,128)S(1)} %get-tuple-element.5) | data formatting | bytes 32768
Async XLA Ops:
  0.6 0.7 %copy-start = (s32[1,8,16]{2,1,0:T(8,128)S(1)}, s32[1,8,16]{2,1,0:T(8,128)}, u32[]{:S(2)}) copy-start(s32[1,8,16]{2,1,0:T(8,128)} %chosen_ref.1) | copy-start | bytes 1540
where the time goes:
time: 35.7 us; the launch traced here: 35.1 us
  Pallas kernels  32.2 us (90%)
  local copies, waits for them, and re-layouts  2.26 us (6%)
  between operations  0.65 us (2%)
    pallas_call x1, Pallas kernels, on_device_fused(): pl.pallas_call(functools.partial(fused_kernel, n), out_shape=(jax.ShapeDt...  32.2 us
    unnamed x4, local copies, waits for them, and re-layouts  2.26 us

commit v1 on v0

--- a/solution.py
+++ b/solution.py
@@ -98,8 +98,8 @@
 
 
 def fused_kernel(
-    n, tokens_hbm, wq_hbm, wk_hbm, wv_hbm, wo_hbm, chosen_ref, mixed_ref, lse_ref,
-    x, wq, wk, wv, wo, q_s, k_s, vt_s, send_k, send_v, got_k, got_v, asked,
+    n, tokens_hbm, wq_hbm, wk_hbm, wv_hbm, wo_hbm, chosen_hbm, mixed_ref, lse_ref,
+    x, wq, wk, wv, wo, chosen_ref, q_s, k_s, vt_s, send_k, send_v, got_k, got_v, asked,
     acc, mx, sm, top, inv, far_s, far_e, att, att_far, wo_far, part,
     load_sem, ask_send, ask_recv, kv_send, kv_recv, part_send, part_recv,
 ):
@@ -114,9 +114,10 @@
 
     loads = []
     for index, (src, dst) in enumerate(
-        ((tokens_hbm.at[0], x), (wk_hbm, wk), (wv_hbm, wv), (wq_hbm, wq), (wo_hbm, wo))
+        ((tokens_hbm.at[0], x), (wk_hbm, wk), (wv_hbm, wv), (wq_hbm, wq), (wo_hbm, wo), (chosen_hbm, chosen_ref))
     ):
         loads.append(pltpu.make_async_copy(src, dst, load_sem.at[index]))
+    loads[5].start()
     loads[0].start()
     loads[1].start()
 
@@ -146,6 +147,7 @@
             device_id={"kv": lax.rem(me + offset, n)}, device_id_type=pl.DeviceIdType.MESH,
         )
 
+    loads[5].wait()
     for offset in range(1, n):
         @pl.when(me >= offset)
         def _():
@@ -193,7 +195,7 @@
 
     loads[0].wait()
     loads[1].wait()
-    for load in loads[2:]:
+    for load in loads[2:5]:
         load.start()
     project(wk, k_s, 1.0)
     select_and_send(0)
@@ -356,6 +358,17 @@
             kv_copy(offset, 1).wait_send()
 
 
+def store_kernel(mixed_ref, lse_ref, mixed_hbm, lse_hbm, sem):
+    copies = [
+        pltpu.make_async_copy(mixed_ref, mixed_hbm, sem.at[0]),
+        pltpu.make_async_copy(lse_ref, lse_hbm, sem.at[1]),
+    ]
+    for copy in copies:
+        copy.start()
+    for copy in copies:
+        copy.wait()
+
+
 def on_device_fused(n, tokens, w_query, w_key, w_value, w_out, chosen):
     _, rows, model = tokens.shape
     width = w_query.shape[1]
@@ -367,13 +380,14 @@
     in_hbm = pl.BlockSpec(memory_space=pltpu.HBM)
     in_vmem = pl.BlockSpec(memory_space=pltpu.VMEM)
     dma = pltpu.SemaphoreType.DMA
-    return pl.pallas_call(
+    chosen = pltpu.with_memory_space_constraint(chosen, pltpu.HBM)
+    mixed, lse = pl.pallas_call(
         functools.partial(fused_kernel, n),
         out_shape=(
-            jax.ShapeDtypeStruct((1, rows // 2, depth), bf16),
-            jax.ShapeDtypeStruct((1, width // HEAD_DIM, rows), f32),
+            pltpu.VMEM((1, rows // 2, depth), bf16),
+            pltpu.VMEM((1, width // HEAD_DIM, rows), f32),
         ),
-        in_specs=[in_hbm] * 5 + [in_vmem],
+        in_specs=[in_hbm] * 6,
         out_specs=(in_vmem, in_vmem),
         scratch_shapes=[
             pltpu.VMEM((rows, model), bf16),
@@ -381,6 +395,7 @@
             pltpu.VMEM((model, width), bf16),
             pltpu.VMEM((model, width), bf16),
             pltpu.VMEM((width, depth), bf16),
+            pltpu.VMEM((1, blocks, picks), jnp.int32),
             pltpu.VMEM((rows, width), bf16),
             pltpu.VMEM((rows, width), bf16),
             pltpu.VMEM((width, rows), bf16),
@@ -400,7 +415,7 @@
             pltpu.VMEM((rows // 2, width), bf16),
             pltpu.VMEM((width, depth), bf16),
             pltpu.VMEM((rows // 2, depth), bf16),
-            dma((5,)),
+            dma((6,)),
             dma((n - 1,)),
             dma((n - 1,)),
             dma((2, n - 1)),
@@ -412,6 +427,19 @@
             collective_id=0, has_side_effects=True, vmem_limit_bytes=53500 * 1024
         ),
     )(tokens, w_query, w_key, w_value, w_out, chosen)
+    mixed = pltpu.with_memory_space_constraint(mixed, pltpu.VMEM)
+    lse = pltpu.with_memory_space_constraint(lse, pltpu.VMEM)
+    return pl.pallas_call(
+        store_kernel,
+        out_shape=(
+            jax.ShapeDtypeStruct(mixed.shape, mixed.dtype),
+            jax.ShapeDtypeStruct(lse.shape, lse.dtype),
+        ),
+        in_specs=[in_vmem] * 2,
+        out_specs=(in_hbm, in_hbm),
+        scratch_shapes=[dma((2,))],
+        compiler_params=pltpu.CompilerParams(vmem_limit_bytes=1024 * 1024),
+    )(mixed, lse)
 
 
 def on_device(tokens, w_query, w_key, w_value, w_out, chosen):

time: 35.7 us -> 34.4 us (0.964)
  local copies, waits for them, and re-layouts: 2.26 us -> 0 us
  Pallas kernels: 32.2 us -> 33.2 us
    unnamed x4 -> x0, local copies, waits for them, and re-layouts: 2.26 us -> none
    pallas_call x1 -> x2, Pallas kernels: 32.2 us -> 33.2 us  [the longest x1 32.2 us: on_device_fused(): pl.pallas_call(functools.partial(fused_kernel, n), out_shape=(pltpu.VMEM(...]
where the time goes in v1:
time: 34.4 us; the launch traced here: 33.9 us
  Pallas kernels  33.2 us (97%)
  between operations  0.64 us (2%)
    pallas_call x1, Pallas kernels, on_device_fused(): pl.pallas_call(functools.partial(fused_kernel, n), out_shape=(pltpu.VMEM(...  32.2 us
    pallas_call x1, Pallas kernels, on_device_fused(): pl.pallas_call(store_kernel, out_shape=(jax.ShapeDtypeStruct(mixed.shape,...  0.99 us

profile of v1, /device:TPU:17, one launch (start us, length us, event | category | flops | bytes accessed | tf_op | source)
XLA Modules:
  0.0 33.9 jit_solution(7721486666945870047)
XLA Ops:
  0.6 32.2 %shard_map.77 = (bf16[1,256,2048]{2,1,0:T(8,128)(2,1)S(1)}, f32[1,8,512]{2,1,0:T(8,128)S(1)}) custom-call(bf16[1,512,2048]{2,1,0:T(8,128)(2,1)} %tokens_hbm.1, bf16[2048,512]{1,0:T(8,128)(2,1)} %wq_hbm.1, bf16[2048,512]{1,0:T(8,128)(2,1)} %wk_hbm.1, bf16[2048,512]{1,0:T(8,128)(2,1)} %wv_hbm.1, bf16[512,2048]{1,0:T(8,128)(2,1)} %wo_hbm.1, s32[1,8,16]{2,1,0:T(8,128)} %chosen_hbm.1), custom_call_target="tpu_custom_call" | custom-call | tf_op jit(solution)/shard_map/pallas_call | solution.py:384
  32.9 1.0 %shard_map.78 = (bf16[1,256,2048]{2,1,0:T(8,128)(2,1)}, f32[1,8,512]{2,1,0:T(8,128)}) custom-call(bf16[1,256,2048]{2,1,0:T(8,128)(2,1)S(1)} %get-tuple-element.4.mixed_ref, f32[1,8,512]{2,1,0:T(8,128)S(1)} %get-tuple-element.5.lse_ref), custom_call_target="tpu_custom_call" | custom-call | tf_op jit(solution)/shard_map/pallas_call | solution.py:432

commit v2 on v0

v2 whole, which is shorter than its diff:
```python
import functools

import jax
import jax.numpy as jnp
from jax import lax
from jax.experimental import pallas as pl
from jax.experimental.pallas import tpu as pltpu
from jax.sharding import PartitionSpec as P

HEAD_DIM = 64
BLOCK = 64


def on_device_general(tokens, w_query, w_key, w_value, w_out, chosen):
    inputs = tokens[0]
    listed = chosen[0]
    tok_rows = inputs.shape[0]
    queries = jnp.dot(inputs, w_query, preferred_element_type=jnp.float32).astype(jnp.bfloat16)
    keys_local = jnp.dot(inputs, w_key, preferred_element_type=jnp.float32).astype(jnp.bfloat16)
    values_local = jnp.dot(inputs, w_value, preferred_element_type=jnp.float32).astype(jnp.bfloat16)
    width = queries.shape[1]
    head_count = width // HEAD_DIM
    span_blocks = tok_rows // BLOCK
    query_count, picks = listed.shape
    myself = lax.axis_index("kv")
    valid = listed >= 0
    key_blocks = keys_local.reshape(span_blocks, BLOCK, width)
    value_blocks = values_local.reshape(span_blocks, BLOCK, width)
    kv_count = lax.axis_size("kv")
    capacity = max(1, min(2, span_blocks // 3))
    owners = jnp.where(valid, listed // span_blocks, myself)
    within = jnp.where(valid, listed % span_blocks, 0)
    foreign = valid & (owners != myself)
    owner_iota = jnp.arange(kv_count, dtype=jnp.int32)
    within_iota = jnp.arange(span_blocks, dtype=jnp.int32)
    hits = (
        (owners[:, :, None, None] == owner_iota[:, None])
        & (within[:, :, None, None] == within_iota[None, :])
        & foreign[:, :, None, None]
    )
    needed = jnp.any(hits, axis=(0, 1))
    order_rank = jnp.cumsum(needed.astype(jnp.int32), axis=1) - 1
    matches = needed[:, None, :] & (
        order_rank[:, None, :] == jnp.arange(capacity, dtype=jnp.int32)[None, :, None]
    )
    wanted = jnp.where(
        jnp.any(matches, axis=2), jnp.sum(matches.astype(jnp.int32) * within_iota, axis=2), -1
    )
    asked = lax.all_to_all(wanted, "kv", split_axis=0, concat_axis=0, tiled=True)
    present = (asked >= 0)[:, :, None, None]
    picked = jnp.clip(asked, 0, span_blocks - 1)
    zero_block = jnp.zeros((), jnp.bfloat16)
    send_keys = jnp.where(present, key_blocks[picked], zero_block)
    send_values = jnp.where(present, value_blocks[picked], zero_block)
    got_keys, got_values = (
        lax.all_to_all(send_keys, "kv", split_axis=0, concat_axis=0, tiled=True),
        lax.all_to_all(send_values, "kv", split_axis=0, concat_axis=0, tiled=True),
    )
    pool_keys = jnp.concatenate([key_blocks, got_keys.reshape(-1, BLOCK, width)], axis=0)
    pool_values = jnp.concatenate([value_blocks, got_values.reshape(-1, BLOCK, width)], axis=0)
    slot_rank = jnp.sum(hits.astype(jnp.int32) * order_rank[None, None], axis=(2, 3))
    slots = jnp.where(foreign, span_blocks + owners * capacity + slot_rank, within)
    keys_sel = pool_keys[slots].reshape(query_count, picks, BLOCK, head_count, HEAD_DIM)
    values_sel = pool_values[slots].reshape(query_count, picks, BLOCK, head_count, HEAD_DIM)
    query_blocks = queries.reshape(query_count, BLOCK, head_count, HEAD_DIM)
    scores = jnp.einsum(
        "nqhd,nskhd->nhqsk", query_blocks, keys_sel, preferred_element_type=jnp.float32
    ) * HEAD_DIM ** (-0.5)
    offsets = jnp.arange(BLOCK, dtype=jnp.int32)
    key_pos = listed[:, :, None] * BLOCK + offsets[None, None, :]
    query_pos = (myself * span_blocks + jnp.arange(query_count, dtype=jnp.int32))[
        :, None
    ] * BLOCK + offsets[None, :]
    allowed = valid[:, None, :, None] & (key_pos[:, None, :, :] <= query_pos[:, :, None, None])
    scores = jnp.where(allowed[:, None], scores, -jnp.inf)
    row_max = jnp.max(scores, axis=(3, 4), keepdims=True)
    exp_terms = jnp.exp(scores - row_max)
    row_sum = jnp.sum(exp_terms, axis=(3, 4), keepdims=True)
    weights = (exp_terms / row_sum).astype(jnp.bfloat16)
    attended = jnp.einsum(
        "nhqsk,nskhd->nqhd", weights, values_sel, preferred_element_type=jnp.float32
    )
    attended = attended.astype(jnp.bfloat16).reshape(tok_rows, width)
    log_sums = (row_max + jnp.log(row_sum))[:, :, :, 0, 0]
    log_sums = jnp.transpose(log_sums, (1, 0, 2)).reshape(head_count, tok_rows)
    mixed = lax.psum_scatter(
        jnp.dot(attended, w_out, preferred_element_type=jnp.float32).astype(jnp.bfloat16),
        "tp",
        scatter_dimension=0,
        tiled=True,
    )
    return (mixed[None], log_sums[None])


CAPACITY = 2
LANES = 128
QTILE = 256
STEP = 256


def fused_kernel(
    n, tokens_hbm, wq_hbm, wk_hbm, wv_hbm, wo_hbm, chosen_hbm, out_ref, last_att_ref, last_wo_ref, lse_ref,
    x, wq, wk, wv, wo, chosen_ref, q_s, k_s, vt_s, hot, send_k, send_v, got_k, got_v, asked,
    acc, mx, sm, inv, keep_inv, far_e, att, att_send,
    load_sem, w_sem, ask_send, ask_recv, kv_send, kv_recv, att_sem_s, att_sem_r, wo_send, wo_recv,
):
    me = lax.axis_index("kv")
    core = lax.axis_index("tp")
    rows, width = q_s.shape
    depth = wo.shape[3]
    half = rows // 2
    blocks = rows // BLOCK
    pairs = width // LANES
    chunks = width // STEP
    per_chunk = STEP // LANES
    foreign_rows = CAPACITY * BLOCK
    last = pairs - 1
    early_pairs = pairs - 2
    bf16, f32 = jnp.bfloat16, jnp.float32
    mesh_ids = pl.DeviceIdType.MESH

    def part(c):
        return slice(c * STEP, (c + 1) * STEP)

    load_chosen = pltpu.make_async_copy(chosen_hbm, chosen_ref, load_sem.at[0])
    load_x = pltpu.make_async_copy(tokens_hbm.at[0], x, load_sem.at[1])
    load_q = pltpu.make_async_copy(wq_hbm, wq, load_sem.at[3])
    weights = ((wk_hbm, wk), (wv_hbm, wv))

    def load_w(which, c):
        src, dst = weights[which]
        return pltpu.make_async_copy(src.at[:, part(c)], dst.at[:, part(c)], w_sem.at[which, c])

    wo_own = pltpu.make_async_copy(wo_hbm, wo.at[:, 0], load_sem.at[2])
    wo_far = pltpu.make_async_remote_copy(
        src_ref=wo_hbm, dst_ref=wo.at[:, 1], send_sem=wo_send, recv_sem=wo_recv,
        device_id={"tp": 1 - core}, device_id_type=mesh_ids,
    )

    load_chosen.start()
    load_x.start()
    load_w(0, 0).start()

    barrier = pltpu.get_barrier_semaphore()
    for offset in range(1, n):
        @pl.when(me + offset < n)
        def _():
            pl.semaphore_signal(barrier, inc=1, device_id={"kv": me + offset}, device_id_type=mesh_ids)
    pl.semaphore_signal(barrier, inc=1, device_id={"tp": 1 - core}, device_id_type=mesh_ids)

    def ask_copy(offset):
        return pltpu.make_async_remote_copy(
            src_ref=chosen_ref, dst_ref=asked.at[offset - 1],
            send_sem=ask_send.at[offset - 1], recv_sem=ask_recv.at[offset - 1],
            device_id={"kv": lax.rem(me + n - offset, n)}, device_id_type=mesh_ids,
        )

    def kv_copy(offset, g, which):
        far = pl.ds((offset - 1) * foreign_rows, foreign_rows)
        group = pl.ds(0, early_pairs) if g == 0 else pl.ds(early_pairs + g - 1, 1)
        return pltpu.make_async_remote_copy(
            src_ref=(send_k, send_v)[which].at[offset - 1, group],
            dst_ref=got_k.at[group, far, :] if which == 0 else got_v.at[group, :, far],
            send_sem=kv_send.at[which, offset - 1, g], recv_sem=kv_recv.at[which, offset - 1, g],
            device_id={"kv": lax.rem(me + offset, n)}, device_id_type=mesh_ids,
        )

    def att_copy(g):
        group = pl.ds(0, early_pairs) if g == 0 else pl.ds(early_pairs + g - 1, 1)
        return pltpu.make_async_remote_copy(
            src_ref=att_send.at[group], dst_ref=att.at[1, group],
            send_sem=att_sem_s.at[g], recv_sem=att_sem_r.at[g],
            device_id={"tp": 1 - core}, device_id_type=mesh_ids,
        )

    load_chosen.wait()
    pl.semaphore_wait(barrier, me + 1)
    for offset in range(1, n):
        @pl.when(me >= offset)
        def _():
            ask_copy(offset).start()
    load_w(1, 0).start()
    load_w(0, 1).start()

    def project_k(c):
        load_w(0, c).wait()
        cols = part(c)
        for r in (slice(0, half), slice(half, rows)):
            k_s[r, cols] = jnp.dot(x[r, :], wk[:, cols], preferred_element_type=f32).astype(bf16)

    def project_v(c):
        load_w(1, c).wait()
        cols = part(c)
        for r in (slice(0, half), slice(half, rows)):
            y = jnp.dot(x[r, :], wv[:, cols], preferred_element_type=f32).astype(bf16)
            vt_s[cols, r] = y.T

    def project_q():
        load_q.wait()

        @pl.loop(0, chunks)
        def _(c):
            cols = pl.ds(pl.multiple_of(c * STEP, STEP), STEP)
            y = jnp.dot(x[...], wq[:, cols], preferred_element_type=f32).astype(bf16)
            q_s[:, cols] = y * jnp.asarray(HEAD_DIM ** (-0.5), bf16)

    def pick(offset):
        ask_copy(offset).wait_recv()
        row = asked[offset - 1, 0, 0:1, :]
        inside = (row >= me * blocks) & (row < (me + 1) * blocks)
        low = jnp.min(jnp.where(inside, row, (me + 1) * blocks - 1), axis=1, keepdims=True)
        high = jnp.max(jnp.where(inside, row, me * blocks), axis=1, keepdims=True)
        low, high = (low - me * blocks) * BLOCK, (high - me * blocks - 1) * BLOCK
        place = lax.broadcasted_iota(jnp.int32, (foreign_rows, rows), 0)
        column = lax.broadcasted_iota(jnp.int32, (foreign_rows, rows), 1)
        want = place + jnp.where(place < BLOCK, low, high)
        hot[offset - 1] = (column == want).astype(f32).astype(bf16)

    def gather_and_send(offset, c, kinds):
        for which in kinds:
            if which == 0:
                y = jnp.dot(hot[offset - 1], k_s[:, part(c)], preferred_element_type=f32).astype(bf16)
            else:
                y = lax.dot_general(
                    vt_s[part(c), :], hot[offset - 1], (((1,), (1,)), ((), ())), preferred_element_type=f32
                ).astype(bf16)
            for i in range(per_chunk):
                here = slice(i * LANES, (i + 1) * LANES)
                if which == 0:
                    send_k[offset - 1, c * per_chunk + i] = y[:, here]
                else:
                    send_v[offset - 1, c * per_chunk + i] = y[here, :]
            if c * per_chunk < early_pairs:
                kv_copy(offset, 0, which).start()
        if c == chunks - 1:
            @pl.when(me + 2 >= n)
            def _():
                for g in (1, 2):
                    for which in kinds:
                        kv_copy(offset, g, which).start()

    def to(offset):
        return pl.when(me + offset < n)

    load_x.wait()
    project_k(0)

    @pl.when((me >= 1) & (me + 1 < n))
    def _():
        pick(1)
        gather_and_send(1, 0, (0,))

    load_w(1, 1).start()
    load_q.start()
    project_v(0)

    @pl.when((me >= 1) & (me + 1 < n))
    def _():
        gather_and_send(1, 0, (1,))

    project_k(1)
    for offset in range(2, n):
        @pl.when((me >= 1) & (me + offset < n))
        def _():
            pick(offset)
            gather_and_send(offset, 0, (0, 1))

    project_v(1)

    @pl.when(me >= 1)
    def _():
        for offset in range(1, n):
            @to(offset)
            def _():
                gather_and_send(offset, 1, (0, 1))

    wo_own.start()
    wo_far.start()
    project_q()

    @pl.when(me == 0)
    def _():
        for offset in range(1, n):
            pick(offset)
            gather_and_send(offset, 0, (0, 1))
        for offset in range(1, n):
            gather_and_send(offset, 1, (0, 1))

    first = lax.broadcasted_iota(jnp.int32, (QTILE, LANES), 1) < HEAD_DIM
    zero = jnp.zeros((), bf16)

    def one_head(q, side):
        return jnp.where(first, q, zero) if side == 0 else jnp.where(first, zero, q)

    def scores_t(k, q):
        return lax.dot_general(k, q, (((1,), (1,)), ((), ())), preferred_element_type=f32)

    def attend(q, k, vt, mask):
        s = scores_t(k, q)
        tail = jnp.where(mask, s[-QTILE:], -jnp.inf)
        s = tail if s.shape[0] == QTILE else jnp.concatenate([s[:-QTILE], tail], axis=0)
        m = jnp.max(s, axis=0, keepdims=True)
        e = jnp.exp(s - m)
        l = jnp.sum(e, axis=0, keepdims=True)
        o = jnp.dot(vt, e.astype(bf16), preferred_element_type=f32)
        return m, l, o

    tri = lax.broadcasted_iota(jnp.int32, (QTILE, QTILE), 0) <= lax.broadcasted_iota(
        jnp.int32, (QTILE, QTILE), 1
    )

    def lanes_of(p):
        return pl.ds(pl.multiple_of(p * LANES, LANES), LANES)

    def of_head(p, side):
        head = 2 * p + side
        return pl.ds(head, 1), pl.ds(pl.multiple_of(head * HEAD_DIM, HEAD_DIM), HEAD_DIM)

    def local(p):
        cols = lanes_of(p)
        for i in range(rows // QTILE):
            here = slice(i * QTILE, (i + 1) * QTILE)
            keys = slice(0, (i + 1) * QTILE)
            q, k = q_s[here, cols], k_s[keys, cols]
            for side in range(2):
                line, wide = of_head(p, side)
                m, l, o = attend(one_head(q, side), k, vt_s[wide, keys], tri)
                mx[line, here] = m
                sm[line, here] = l
                acc[wide, here] = o

    def throttled(act):
        @pl.when(me + 2 < n)
        def _():
            for offset in range(n - 1, 0, -1):
                @to(offset)
                def _():
                    act(offset)

    def start_held(offset):
        for which in range(2):
            kv_copy(offset, 1, which).start()

    pl.loop(0, pairs // 2)(local)
    throttled(start_held)
    pl.loop(pairs // 2, pairs)(local)

    def move_on(which):
        def act(offset):
            kv_copy(offset, 1, which).wait_send()
            kv_copy(offset, 2, which).start()

        return act

    def arrive(g, which, count):
        for offset in range(1, count + 1):
            kv_copy(offset, g, which).wait_recv()

    def weigh(p, count):
        far = count * foreign_rows
        for i in range(rows // QTILE):
            here = slice(i * QTILE, (i + 1) * QTILE)
            for side in range(2):
                line, _ = of_head(p, side)
                m, l = mx[line, here], sm[line, here]
                if count:
                    s = scores_t(got_k[p, :far, :], one_head(q_s[here, lanes_of(p)], side))
                    t = jnp.maximum(m, jnp.max(s, axis=0, keepdims=True))
                    e = jnp.exp(s - t)
                    k = jnp.exp(m - t)
                    l = l * k + jnp.sum(e, axis=0, keepdims=True)
                    far_e[side, :far, here] = e.astype(bf16)
                    m = t
                r = 1.0 / l
                inv[line, here] = r
                keep_inv[line, here] = k * r if count else r
                lse_ref[0, line, here] = m + jnp.log(l)

    theirs = pl.ds(pl.multiple_of((1 - core) * half, half), half)
    mine = pl.ds(pl.multiple_of(core * half, half), half)

    def blend(p, count, send=None):
        far = count * foreign_rows
        for cols in (theirs, mine):
            heads = []
            for side in range(2):
                line, wide = of_head(p, side)
                o = acc[wide, cols] * keep_inv[line, cols]
                if count:
                    vt = got_v[p, side * HEAD_DIM:(side + 1) * HEAD_DIM, :far]
                    o = o + jnp.dot(vt, far_e[side, :far, cols], preferred_element_type=f32) * inv[line, cols]
                heads.append(o.astype(bf16))
            block = jnp.concatenate(heads, axis=0).T
            if cols is theirs:
                att_send[p] = block
                if send is not None:
                    att_copy(send).start()
            else:
                att[0, p] = block

    def each_count(act):
        for count in range(n):
            @pl.when(me == count)
            def _():
                act(count)

    def early(count):
        arrive(0, 0, count)
        arrive(0, 1, count)

        @pl.loop(0, early_pairs)
        def _(p):
            weigh(p, count)
            blend(p, count)

    def middle(count):
        arrive(1, 0, count)
        weigh(last - 1, count)
        arrive(1, 1, count)
        blend(last - 1, count, 1)

    def weigh_last(count):
        arrive(2, 0, count)
        weigh(last, count)

    def blend_last(count):
        arrive(2, 1, count)
        blend(last, count, 2)

    each_count(early)
    att_copy(0).start()
    throttled(move_on(0))
    each_count(middle)
    throttled(move_on(1))

    wo_own.wait()
    wo_far.wait_recv()
    last_wo_ref[...] = wo[last].reshape(2 * LANES, depth)
    each_count(weigh_last)

    for g in range(2):
        att_copy(g).wait_recv()
    step = depth // 4
    for c in range(4):
        cols = slice(c * step, (c + 1) * step)
        rows_of = jnp.concatenate([att[side, p] for p in range(last) for side in range(2)], axis=1)
        out_ref[:, cols] = jnp.dot(
            rows_of, wo[:last, :, :, cols].reshape(2 * last * LANES, step), preferred_element_type=f32
        )

    each_count(blend_last)
    att_copy(2).wait_recv()
    last_att_ref[...] = jnp.concatenate([att[0, last], att[1, last]], axis=1)

    for g in range(3):
        att_copy(g).wait_send()
    wo_far.wait_send()
    for offset in range(1, n):
        @pl.when(me >= offset)
        def _():
            ask_copy(offset).wait_send()

        @to(offset)
        def _():
            for which in range(2):
                for g in (0, 2):
                    kv_copy(offset, g, which).wait_send()

                @pl.when(me + 2 >= n)
                def _():
                    kv_copy(offset, 1, which).wait_send()


def final_kernel(part_ref, att_ref, wo_ref, lse_ref, mixed_hbm, lse_hbm, out, sem):
    lse_copy = pltpu.make_async_copy(lse_ref, lse_hbm, sem.at[4])
    lse_copy.start()
    step = out.shape[1] // 4
    copies = []
    for c in range(4):
        cols = slice(c * step, (c + 1) * step)
        out[:, cols] = (
            part_ref[:, cols] + jnp.dot(att_ref[...], wo_ref[:, cols], preferred_element_type=jnp.float32)
        ).astype(out.dtype)
        copies.append(pltpu.make_async_copy(out.at[:, cols], mixed_hbm.at[0, :, cols], sem.at[c]))
        copies[-1].start()
    for copy in copies:
        copy.wait()
    lse_copy.wait()


def on_device_fused(n, tokens, w_query, w_key, w_value, w_out, chosen):
    _, rows, model = tokens.shape
    width = w_query.shape[1]
    depth = w_out.shape[1]
    blocks, picks = chosen.shape[1:]
    foreign_rows = CAPACITY * BLOCK
    heads = width // HEAD_DIM
    pairs = width // LANES
    half = rows // 2
    bf16, f32 = jnp.bfloat16, jnp.float32
    in_hbm = pl.BlockSpec(memory_space=pltpu.HBM)
    in_vmem = pl.BlockSpec(memory_space=pltpu.VMEM)
    dma = pltpu.SemaphoreType.DMA
    operands = [
        pltpu.with_memory_space_constraint(a, pltpu.HBM)
        for a in (tokens, w_query, w_key, w_value, w_out.reshape(pairs, LANES, depth), chosen)
    ]
    parts = pl.pallas_call(
        functools.partial(fused_kernel, n),
        out_shape=(
            pltpu.VMEM((half, depth), f32),
            pltpu.VMEM((half, 2 * LANES), bf16),
            pltpu.VMEM((2 * LANES, depth), bf16),
            pltpu.VMEM((1, heads, rows), f32),
        ),
        in_specs=[in_hbm] * 6,
        out_specs=(in_vmem,) * 4,
        scratch_shapes=[
            pltpu.VMEM((rows, model), bf16),
            pltpu.VMEM((model, width), bf16),
            pltpu.VMEM((model, width), bf16),
            pltpu.VMEM((model, width), bf16),
            pltpu.VMEM((pairs, 2, LANES, depth), bf16),
            pltpu.VMEM((1, blocks, picks), jnp.int32),
            pltpu.VMEM((rows, width), bf16),
            pltpu.VMEM((rows, width), bf16),
            pltpu.VMEM((width, rows), bf16),
            pltpu.VMEM((n - 1, foreign_rows, rows), bf16),
            pltpu.VMEM((n - 1, pairs, foreign_rows, LANES), bf16),
            pltpu.VMEM((n - 1, pairs, LANES, foreign_rows), bf16),
            pltpu.VMEM((pairs, (n - 1) * foreign_rows, LANES), bf16),
            pltpu.VMEM((pairs, LANES, (n - 1) * foreign_rows), bf16),
            pltpu.VMEM((n - 1, 1, blocks, picks), jnp.int32),
            pltpu.VMEM((width, rows), f32),
            pltpu.VMEM((heads, rows), f32),
            pltpu.VMEM((heads, rows), f32),
            pltpu.VMEM((heads, rows), f32),
            pltpu.VMEM((heads, rows), f32),
            pltpu.VMEM((2, (n - 1) * foreign_rows, rows), bf16),
            pltpu.VMEM((2, pairs, half, LANES), bf16),
            pltpu.VMEM((pairs, half, LANES), bf16),
            dma((4,)),
            dma((2, 2)),
            dma((n - 1,)),
            dma((n - 1,)),
            dma((2, n - 1, 3)),
            dma((2, n - 1, 3)),
            dma((3,)),
            dma((3,)),
            dma,
            dma,
        ],
        compiler_params=pltpu.CompilerParams(
            collective_id=0, has_side_effects=True, vmem_limit_bytes=40 * 1024 * 1024
        ),
    )(*operands)
    return pl.pallas_call(
        final_kernel,
        out_shape=(
            jax.ShapeDtypeStruct((1, half, depth), bf16),
            jax.ShapeDtypeStruct((1, heads, rows), f32),
        ),
        in_specs=[in_vmem] * 4,
        out_specs=(in_hbm, in_hbm),
        scratch_shapes=[pltpu.VMEM((half, depth), bf16), dma((5,))],
        compiler_params=pltpu.CompilerParams(vmem_limit_bytes=4 * 1024 * 1024),
    )(*[pltpu.with_memory_space_constraint(a, pltpu.VMEM) for a in parts])


def on_device(tokens, w_query, w_key, w_value, w_out, chosen):
    n, cores = lax.axis_size("kv"), lax.axis_size("tp")
    rows, width = tokens.shape[1], w_query.shape[1]
    blocks, picks = chosen.shape[1:]
    full_rows = blocks - 1 + CAPACITY * (n - 1) <= picks - 1
    fits = rows == 2 * QTILE and width == 2 * STEP and blocks >= 3 * CAPACITY
    if full_rows and fits and cores == 2 and n > 1:
        return on_device_fused(n, tokens, w_query, w_key, w_value, w_out, chosen)
    return on_device_general(tokens, w_query, w_key, w_value, w_out, chosen)


def solution(mesh):
    return jax.shard_map(
        on_device,
        mesh=mesh,
        in_specs=(
            P("dp", "kv", None),
            P(None, "tp"),
            P(None, "tp"),
            P(None, "tp"),
            P("tp", None),
            P("dp", "kv", None),
        ),
        out_specs=(P("dp", ("kv", "tp"), None), P("dp", "tp", "kv")),
        check_vma=False,
    )
```

time: 35.7 us -> 32.3 us (0.905); the launches traced: 35.1 us -> 32.1 us
  local copies, waits for them, and re-layouts: 2.26 us -> 0 us
  Pallas kernels: 32.2 us -> 31.5 us
    unnamed x4 -> x0, local copies, waits for them, and re-layouts: 2.26 us -> none
    pallas_call x1 -> x2, Pallas kernels: 32.2 us -> 31.5 us  [the longest x1 30.2 us: on_device_fused(): pl.pallas_call(functools.partial(fused_kernel, n), out_shape=(pltpu.VMEM(...]
where the time goes in v2:
time: 32.3 us; the launch traced here: 32.1 us
  Pallas kernels  31.5 us (98%)
  between operations  0.64 us (2%)
    pallas_call x1, Pallas kernels, on_device_fused(): pl.pallas_call(functools.partial(fused_kernel, n), out_shape=(pltpu.VMEM(...  30.2 us
    pallas_call x1, Pallas kernels, on_device_fused(): pl.pallas_call(final_kernel, out_shape=(jax.ShapeDtypeStruct((1, half, de...  1.25 us

profile of v2, /device:TPU:17, one launch (start us, length us, event | category | flops | bytes accessed | tf_op | source)
XLA Modules:
  0.0 32.1 jit_solution(8816492205992467456)
XLA Ops:
  0.6 30.2 %shard_map.77 = (f32[256,2048]{1,0:T(8,128)S(1)}, bf16[256,256]{1,0:T(8,128)(2,1)S(1)}, bf16[256,2048]{1,0:T(8,128)(2,1)S(1)}, f32[1,8,512]{2,1,0:T(8,128)S(1)}) custom-call(bf16[1,512,2048]{2,1,0:T(8,128)(2,1)} %tokens_hbm.1, bf16[2048,512]{1,0:T(8,128)(2,1)} %wq_hbm.1, bf16[2048,512]{1,0:T(8,128)(2,1)} %wk_hbm.1, bf16[2048,512]{1,0:T(8,128)(2,1)} %wv_hbm.1, ...), custom_call_target="tpu_custom_call" | custom-call | tf_op jit(solution)/shard_map/pallas_call | solution.py:508
  30.9 1.2 %shard_map.78 = (bf16[1,256,2048]{2,1,0:T(8,128)(2,1)}, f32[1,8,512]{2,1,0:T(8,128)}) custom-call(f32[256,2048]{1,0:T(8,128)S(1)} %get-tuple-element.6.part_ref, bf16[256,256]{1,0:T(8,128)(2,1)S(1)} %get-tuple-element.7.att_ref, bf16[256,2048]{1,0:T(8,128)(2,1)S(1)} %get-tuple-element.8.wo_ref, f32[1,8,512]{2,1,0:T(8,128)S(1)} %get-tuple-element.9.lse_ref), custom_call_target="tpu_custom_call" | custom-call | tf_op jit(solution)/shard_map/pallas_call | solution.py:557

commit v3 on v2

--- a/solution.py
+++ b/solution.py
@@ -332,25 +332,22 @@
     def throttled(act):
         @pl.when(me + 2 < n)
         def _():
-            for offset in range(n - 1, 0, -1):
-                @to(offset)
-                def _():
-                    act(offset)
-
-    def start_held(offset):
-        for which in range(2):
-            kv_copy(offset, 1, which).start()
+            for which in range(2):
+                for offset in range(n - 1, 0, -1):
+                    @to(offset)
+                    def _():
+                        act(offset, which)
+
+    def start_held(offset, which):
+        kv_copy(offset, 1, which).start()
 
     pl.loop(0, pairs // 2)(local)
     throttled(start_held)
     pl.loop(pairs // 2, pairs)(local)
 
-    def move_on(which):
-        def act(offset):
-            kv_copy(offset, 1, which).wait_send()
-            kv_copy(offset, 2, which).start()
-
-        return act
+    def move_on(offset, which):
+        kv_copy(offset, 1, which).wait_send()
+        kv_copy(offset, 2, which).start()
 
     def arrive(g, which, count):
         for offset in range(1, count + 1):
@@ -429,15 +426,15 @@
 
     each_count(early)
     att_copy(0).start()
-    throttled(move_on(0))
+    throttled(move_on)
     each_count(middle)
-    throttled(move_on(1))
 
     wo_own.wait()
     wo_far.wait_recv()
     last_wo_ref[...] = wo[last].reshape(2 * LANES, depth)
     each_count(weigh_last)
 
+    each_count(blend_last)
     for g in range(2):
         att_copy(g).wait_recv()
     step = depth // 4
@@ -448,7 +445,6 @@
             rows_of, wo[:last, :, :, cols].reshape(2 * last * LANES, step), preferred_element_type=f32
         )
 
-    each_count(blend_last)
     att_copy(2).wait_recv()
     last_att_ref[...] = jnp.concatenate([att[0, last], att[1, last]], axis=1)
 
@@ -472,19 +468,16 @@
 
 
 def final_kernel(part_ref, att_ref, wo_ref, lse_ref, mixed_hbm, lse_hbm, out, sem):
-    lse_copy = pltpu.make_async_copy(lse_ref, lse_hbm, sem.at[4])
+    lse_copy = pltpu.make_async_copy(lse_ref, lse_hbm, sem.at[1])
     lse_copy.start()
     step = out.shape[1] // 4
-    copies = []
     for c in range(4):
         cols = slice(c * step, (c + 1) * step)
         out[:, cols] = (
             part_ref[:, cols] + jnp.dot(att_ref[...], wo_ref[:, cols], preferred_element_type=jnp.float32)
         ).astype(out.dtype)
-        copies.append(pltpu.make_async_copy(out.at[:, cols], mixed_hbm.at[0, :, cols], sem.at[c]))
-        copies[-1].start()
-    for copy in copies:
-        copy.wait()
+        pltpu.make_async_copy(out.at[:, cols], mixed_hbm.at[0, :, cols], sem.at[0]).start()
+    pltpu.make_async_copy(out, mixed_hbm.at[0], sem.at[0]).wait()
     lse_copy.wait()
 
 
@@ -562,7 +555,7 @@
         ),
         in_specs=[in_vmem] * 4,
         out_specs=(in_hbm, in_hbm),
-        scratch_shapes=[pltpu.VMEM((half, depth), bf16), dma((5,))],
+        scratch_shapes=[pltpu.VMEM((half, depth), bf16), dma((2,))],
         compiler_params=pltpu.CompilerParams(vmem_limit_bytes=4 * 1024 * 1024),
     )(*[pltpu.with_memory_space_constraint(a, pltpu.VMEM) for a in parts])
 

time: 32.3 us -> 31.7 us (0.981)
  Pallas kernels: 31.5 us -> 30.8 us
    pallas_call x1, Pallas kernels: 30.2 us -> 29.5 us  [on_device_fused(): pl.pallas_call(functools.partial(fused_kernel, n), out_shape=(pltpu.VMEM(...]
where the time goes in v3:
time: 31.7 us; the launch traced here: 31.4 us
  Pallas kernels  30.8 us (97%)
  between operations  0.64 us (2%)
    pallas_call x1, Pallas kernels, on_device_fused(): pl.pallas_call(functools.partial(fused_kernel, n), out_shape=(pltpu.VMEM(...  29.5 us
    pallas_call x1, Pallas kernels, on_device_fused(): pl.pallas_call(final_kernel, out_shape=(jax.ShapeDtypeStruct((1, half, de...  1.22 us

profile of v3, /device:TPU:17, one launch (start us, length us, event | category | flops | bytes accessed | tf_op | source)
XLA Modules:
  0.0 31.4 jit_solution(8665524969582968969)
XLA Ops:
  0.6 29.5 %shard_map.77 = (f32[256,2048]{1,0:T(8,128)S(1)}, bf16[256,256]{1,0:T(8,128)(2,1)S(1)}, bf16[256,2048]{1,0:T(8,128)(2,1)S(1)}, f32[1,8,512]{2,1,0:T(8,128)S(1)}) custom-call(bf16[1,512,2048]{2,1,0:T(8,128)(2,1)} %tokens_hbm.1, bf16[2048,512]{1,0:T(8,128)(2,1)} %wq_hbm.1, bf16[2048,512]{1,0:T(8,128)(2,1)} %wk_hbm.1, bf16[2048,512]{1,0:T(8,128)(2,1)} %wv_hbm.1, ...), custom_call_target="tpu_custom_call" | custom-call | tf_op jit(solution)/shard_map/pallas_call | solution.py:501
  30.2 1.2 %shard_map.78 = (bf16[1,256,2048]{2,1,0:T(8,128)(2,1)}, f32[1,8,512]{2,1,0:T(8,128)}) custom-call(f32[256,2048]{1,0:T(8,128)S(1)} %get-tuple-element.6.part_ref, bf16[256,256]{1,0:T(8,128)(2,1)S(1)} %get-tuple-element.7.att_ref, bf16[256,2048]{1,0:T(8,128)(2,1)S(1)} %get-tuple-element.8.wo_ref, f32[1,8,512]{2,1,0:T(8,128)S(1)} %get-tuple-element.9.lse_ref), custom_call_target="tpu_custom_call" | custom-call | tf_op jit(solution)/shard_map/pallas_call | solution.py:550

commit v4 on v3

--- a/solution.py
+++ b/solution.py
@@ -102,7 +102,7 @@
     n, tokens_hbm, wq_hbm, wk_hbm, wv_hbm, wo_hbm, chosen_hbm, out_ref, last_att_ref, last_wo_ref, lse_ref,
     x, wq, wk, wv, wo, chosen_ref, q_s, k_s, vt_s, hot, send_k, send_v, got_k, got_v, asked,
     acc, mx, sm, inv, keep_inv, far_e, att, att_send,
-    load_sem, w_sem, ask_send, ask_recv, kv_send, kv_recv, att_sem_s, att_sem_r, wo_send, wo_recv,
+    load_sem, w_sem, ask_send, ask_recv, held_send, bulk_send, kv_recv, att_sem_s, att_sem_r, wo_send, wo_recv,
 ):
     me = lax.axis_index("kv")
     core = lax.axis_index("tp")
@@ -124,14 +124,15 @@
 
     load_chosen = pltpu.make_async_copy(chosen_hbm, chosen_ref, load_sem.at[0])
     load_x = pltpu.make_async_copy(tokens_hbm.at[0], x, load_sem.at[1])
-    load_q = pltpu.make_async_copy(wq_hbm, wq, load_sem.at[3])
+    load_q = pltpu.make_async_copy(wq_hbm, wq, load_sem.at[0])
     weights = ((wk_hbm, wk), (wv_hbm, wv))
 
     def load_w(which, c):
         src, dst = weights[which]
-        return pltpu.make_async_copy(src.at[:, part(c)], dst.at[:, part(c)], w_sem.at[which, c])
-
-    wo_own = pltpu.make_async_copy(wo_hbm, wo.at[:, 0], load_sem.at[2])
+        slot = ((0, 2), (1, 0))[which][c]
+        return pltpu.make_async_copy(src.at[:, part(c)], dst.at[:, part(c)], w_sem.at[slot])
+
+    wo_own = pltpu.make_async_copy(wo_hbm, wo.at[:, 0], load_sem.at[1])
     wo_far = pltpu.make_async_remote_copy(
         src_ref=wo_hbm, dst_ref=wo.at[:, 1], send_sem=wo_send, recv_sem=wo_recv,
         device_id={"tp": 1 - core}, device_id_type=mesh_ids,
@@ -151,7 +152,7 @@
     def ask_copy(offset):
         return pltpu.make_async_remote_copy(
             src_ref=chosen_ref, dst_ref=asked.at[offset - 1],
-            send_sem=ask_send.at[offset - 1], recv_sem=ask_recv.at[offset - 1],
+            send_sem=ask_send, recv_sem=ask_recv.at[offset - 1],
             device_id={"kv": lax.rem(me + n - offset, n)}, device_id_type=mesh_ids,
         )
 
@@ -161,7 +162,8 @@
         return pltpu.make_async_remote_copy(
             src_ref=(send_k, send_v)[which].at[offset - 1, group],
             dst_ref=got_k.at[group, far, :] if which == 0 else got_v.at[group, :, far],
-            send_sem=kv_send.at[which, offset - 1, g], recv_sem=kv_recv.at[which, offset - 1, g],
+            send_sem=held_send.at[which, offset - 1] if g == 1 else bulk_send.at[which, g // 2],
+            recv_sem=kv_recv.at[which, g],
             device_id={"kv": lax.rem(me + offset, n)}, device_id_type=mesh_ids,
         )
 
@@ -350,8 +352,11 @@
         kv_copy(offset, 2, which).start()
 
     def arrive(g, which, count):
-        for offset in range(1, count + 1):
-            kv_copy(offset, g, which).wait_recv()
+        if count:
+            far = pl.ds(0, count * foreign_rows)
+            group = pl.ds(0, early_pairs) if g == 0 else pl.ds(early_pairs + g - 1, 1)
+            landed = got_k.at[group, far, :] if which == 0 else got_v.at[group, :, far]
+            pltpu.make_async_copy(landed, landed, kv_recv.at[which, g]).wait()
 
     def weigh(p, count):
         far = count * foreign_rows
@@ -451,20 +456,24 @@
     for g in range(3):
         att_copy(g).wait_send()
     wo_far.wait_send()
-    for offset in range(1, n):
-        @pl.when(me >= offset)
+    for count in range(1, n):
+        @pl.when(me == count)
         def _():
-            ask_copy(offset).wait_send()
-
-        @to(offset)
+            asks = asked.at[pl.ds(0, count)]
+            pltpu.make_async_copy(asks, asks, ask_send).wait()
+
+        @pl.when(me + count == n - 1)
         def _():
             for which in range(2):
-                for g in (0, 2):
-                    kv_copy(offset, g, which).wait_send()
-
-                @pl.when(me + 2 >= n)
-                def _():
-                    kv_copy(offset, 1, which).wait_send()
+                sent = (send_k, send_v)[which]
+                for g, group in ((0, pl.ds(0, early_pairs)), (1, pl.ds(last, 1))):
+                    gone = sent.at[pl.ds(0, count), group]
+                    pltpu.make_async_copy(gone, gone, bulk_send.at[which, g]).wait()
+
+    @pl.when(me + 2 == n)
+    def _():
+        for which in range(2):
+            kv_copy(1, 1, which).wait_send()
 
 
 def final_kernel(part_ref, att_ref, wo_ref, lse_ref, mixed_hbm, lse_hbm, out, sem):
@@ -532,12 +541,13 @@
             pltpu.VMEM((2, (n - 1) * foreign_rows, rows), bf16),
             pltpu.VMEM((2, pairs, half, LANES), bf16),
             pltpu.VMEM((pairs, half, LANES), bf16),
-            dma((4,)),
+            dma((2,)),
+            dma((3,)),
+            dma,
+            dma((n - 1,)),
+            dma((2, n - 1)),
             dma((2, 2)),
-            dma((n - 1,)),
-            dma((n - 1,)),
-            dma((2, n - 1, 3)),
-            dma((2, n - 1, 3)),
+            dma((2, 3)),
             dma((3,)),
             dma((3,)),
             dma,

time: 31.7 us -> 31.5 us (level)
  no operation moved by 1% of the time
where the time goes in v4:
time: 31.5 us; the launch traced here: 31.2 us
  Pallas kernels  30.5 us (97%)
  between operations  0.64 us (2%)
    pallas_call x1, Pallas kernels, on_device_fused(): pl.pallas_call(functools.partial(fused_kernel, n), out_shape=(pltpu.VMEM(...  29.3 us
    pallas_call x1, Pallas kernels, on_device_fused(): pl.pallas_call(final_kernel, out_shape=(jax.ShapeDtypeStruct((1, half, de...  1.22 us

profile of v4, /device:TPU:17, one launch (start us, length us, event | category | flops | bytes accessed | tf_op | source)
XLA Modules:
  0.0 31.2 jit_solution(7839253126896743365)
XLA Ops:
  0.6 29.3 %shard_map.77 = (f32[256,2048]{1,0:T(8,128)S(1)}, bf16[256,256]{1,0:T(8,128)(2,1)S(1)}, bf16[256,2048]{1,0:T(8,128)(2,1)S(1)}, f32[1,8,512]{2,1,0:T(8,128)S(1)}) custom-call(bf16[1,512,2048]{2,1,0:T(8,128)(2,1)} %tokens_hbm.1, bf16[2048,512]{1,0:T(8,128)(2,1)} %wq_hbm.1, bf16[2048,512]{1,0:T(8,128)(2,1)} %wk_hbm.1, bf16[2048,512]{1,0:T(8,128)(2,1)} %wv_hbm.1, ...), custom_call_target="tpu_custom_call" | custom-call | tf_op jit(solution)/shard_map/pallas_call | solution.py:510
  29.9 1.2 %shard_map.78 = (bf16[1,256,2048]{2,1,0:T(8,128)(2,1)}, f32[1,8,512]{2,1,0:T(8,128)}) custom-call(f32[256,2048]{1,0:T(8,128)S(1)} %get-tuple-element.6.part_ref, bf16[256,256]{1,0:T(8,128)(2,1)S(1)} %get-tuple-element.7.att_ref, bf16[256,2048]{1,0:T(8,128)(2,1)S(1)} %get-tuple-element.8.wo_ref, f32[1,8,512]{2,1,0:T(8,128)S(1)} %get-tuple-element.9.lse_ref), custom_call_target="tpu_custom_call" | custom-call | tf_op jit(solution)/shard_map/pallas_call | solution.py:560
